TPU v7x, 32 devices: a whole 2x2x4 slice. The times are simulated.
32 devices in a mesh: kv: 4 (over y, x), tp: 8 (over z, core).
Axes of the slice: x: 2, y: 2, z: 4, core: 2. Of those that a mesh axis runs over, the one named last changes fastest.
Arguments:
- tokens: bfloat16 [3, 4096], P(None, ('kv', 'tp')), may hold values from -40 to 40
- lengths: int32 [3], replicated, may hold values from 1 to 8192, as said below
- attn_gain: float32 [4096], P(('kv', 'tp')), may hold values from 0.1 to 1.9
- w_query: bfloat16 [4096, 2048], P('kv', 'tp'), may hold values from -0.09375 to 0.09375
- w_key: bfloat16 [4096, 128], P('kv'), may hold values from -0.09375 to 0.09375
- w_value: bfloat16 [4096, 128], P('kv'), may hold values from -0.09375 to 0.09375
- w_forget: bfloat16 [4096, 32], replicated, may hold values from -0.09375 to 0.09375
- forget_bias: float32 [32], replicated, may hold values from -4 to 0
- cache_keys: bfloat16 [3, 128, 8192], P(None, None, ('kv', 'tp')), may hold values from -320 to 320
- cache_values: bfloat16 [3, 128, 8192], P(None, None, ('kv', 'tp')), may hold values from -6 to 6
- cache_decay: float32 [3, 32, 8192], P(None, None, ('kv', 'tp')), may hold values from -1028 to 0, as said below
- out_gain: float32 [2048], replicated, may hold values from 0.1 to 1.9
- w_out: bfloat16 [2048, 4096], P('tp', 'kv'), may hold values from -0.125 to 0.125
- mlp_gain: float32 [4096], P(('kv', 'tp')), may hold values from 0.1 to 1.9
- w_gate: bfloat16 [4096, 11264], P('kv', 'tp'), may hold values from -0.09375 to 0.09375
- w_up: bfloat16 [4096, 11264], P('kv', 'tp'), may hold values from -0.09375 to 0.09375
- w_down: bfloat16 [11264, 4096], P('tp', 'kv'), may hold values from -0.0546875 to 0.0546875
Outputs:
- layer_out: bfloat16 [3, 4096], P(None, ('kv', 'tp'))
Inputs may be any that keep to these rules, and one draw needn't show every extreme that they name: Sequence b has lengths[b] live cache positions, 0 to lengths[b] - 1; some sequence has exactly 8192 in every draw. On live positions, cache_decay[b, h, j] is the sum of the log forget gates of sequence b and head h over positions j + 1 to lengths[b] - 1, so it is zero at the last live position and never rises toward earlier positions; it is zero beyond lengths[b].
All inputs are finite; a program needn't handle non-finite values.
Results may differ from a plain program's by a relative error of at most 0.013.
Values may be sent and summed in bfloat16 or wider, within the bound.
A program may use at most 64 MiB of HBM per device.

v0:
```python
import jax
import jax.numpy as jnp
from jax import lax
from jax.sharding import PartitionSpec as P

QUERY_HEAD_COUNT = 32
HD = 64
KV_HEADS = 2


epsilon = 1e-06
masked_score = -1e30


def spread_rows(share, gain):
    scaled = (share.astype(jnp.float32) * gain).astype(jnp.bfloat16)
    squares = jnp.sum(jnp.square(share.astype(jnp.float32)), axis=1)
    row_block = lax.all_gather(scaled, "tp", axis=1, tiled=True)
    square_total = lax.psum(squares, ("kv", "tp"))
    return (row_block, square_total)


def body(
    tokens,
    lengths,
    attn_gain,
    w_query,
    w_key,
    w_value,
    w_forget,
    forget_bias,
    cache_keys,
    cache_values,
    cache_decay,
    out_gain,
    w_out,
    mlp_gain,
    w_gate,
    w_up,
    w_down,
):
    full_width = tokens.shape[1] * lax.axis_size("kv") * lax.axis_size("tp")
    kv_index = lax.axis_index("kv")
    tp_index = lax.axis_index("tp")
    row_block, square_total = spread_rows(tokens, attn_gain)
    block_rows = row_block.shape[1]
    forget_rows = lax.dynamic_slice_in_dim(w_forget, kv_index * block_rows, block_rows, 0)
    query_part = jnp.dot(row_block, w_query, preferred_element_type=jnp.float32)
    key_part = jnp.dot(row_block, w_key, preferred_element_type=jnp.float32)
    value_part = jnp.dot(row_block, w_value, preferred_element_type=jnp.float32)
    forget_part = jnp.dot(row_block, forget_rows, preferred_element_type=jnp.float32)
    query_sum, key_sum, value_sum, forget_sum = lax.psum(
        (query_part, key_part, value_part, forget_part), "kv"
    )
    first_rms = lax.rsqrt(square_total / full_width + epsilon)[:, None]
    query_local = (query_sum * first_rms).astype(jnp.bfloat16)
    key_new = (key_sum * first_rms).astype(jnp.bfloat16)
    value_new = (value_sum * first_rms).astype(jnp.bfloat16)
    log_gate = jax.nn.log_sigmoid(forget_sum * first_rms + forget_bias)
    query_all = lax.all_gather(query_local, "tp", axis=1, tiled=True)
    batch_rows, key_dims, span = cache_keys.shape
    groups = QUERY_HEAD_COUNT // KV_HEADS
    score_scale = HD ** (-0.5)
    query_grouped = query_all.reshape(batch_rows, KV_HEADS, groups, HD)
    keys_grouped = cache_keys.reshape(batch_rows, KV_HEADS, HD, span)
    values_grouped = cache_values.reshape(batch_rows, KV_HEADS, HD, span)
    scores = jnp.einsum(
        "bkgd,bkdj->bkgj", query_grouped, keys_grouped, preferred_element_type=jnp.float32
    ).reshape(batch_rows, QUERY_HEAD_COUNT, span)
    scores = scores * score_scale + cache_decay + log_gate[:, :, None]
    first_slot = (kv_index * lax.axis_size("tp") + tp_index) * span
    token_positions = first_slot + lax.iota(jnp.int32, span)
    is_live = (token_positions[None, :] < lengths[:, None])[:, None, :]
    scores = jnp.where(is_live, scores, masked_score)
    own_score = (
        jnp.einsum(
            "inpo,ino->inp",
            query_grouped,
            key_new.reshape(batch_rows, KV_HEADS, HD),
            preferred_element_type=jnp.float32,
        ).reshape(batch_rows, QUERY_HEAD_COUNT)
        * score_scale
    )
    local_top = jnp.maximum(jnp.max(scores, axis=2), own_score)
    head_count = w_out.shape[0] // HD
    head_start = tp_index * head_count
    score_top = lax.pmax(local_top, ("kv", "tp"))
    weights = jnp.where(is_live, jnp.exp(scores - score_top[:, :, None]), 0.0)
    weight_total = jnp.sum(weights, axis=2)
    rounded = weights.astype(jnp.bfloat16).reshape(batch_rows, KV_HEADS, groups, span)
    value_sums = jnp.einsum(
        "bkgj,bkdj->bkgd", rounded, values_grouped, preferred_element_type=jnp.float32
    ).reshape(batch_rows, QUERY_HEAD_COUNT, HD)
    weight_total, value_sums = (weight_total, value_sums)
    weight_total, value_sums = (
        lax.psum_scatter(weight_total, "tp", scatter_dimension=1, tiled=True),
        lax.psum_scatter(value_sums, "tp", scatter_dimension=1, tiled=True),
    )
    weight_total, value_sums = lax.psum((weight_total, value_sums), "kv")
    score_top = lax.dynamic_slice_in_dim(score_top, head_start, head_count, 1)
    own_here = lax.dynamic_slice_in_dim(own_score, head_start, head_count, 1)
    new_values = jnp.repeat(value_new.reshape(batch_rows, KV_HEADS, HD), groups, axis=1)
    new_values = lax.dynamic_slice_in_dim(new_values, head_start, head_count, 1).astype(jnp.float32)
    own_weight = jnp.exp(own_here - score_top)
    heads_out = (value_sums + own_weight[:, :, None] * new_values) / (weight_total + own_weight)[
        :, :, None
    ]
    head_gains = lax.dynamic_slice_in_dim(out_gain, head_start * HD, head_count * HD, 0).reshape(
        head_count, HD
    )
    normed = (
        heads_out
        * lax.rsqrt(jnp.mean(jnp.square(heads_out), axis=2, keepdims=True) + epsilon)
        * head_gains
    )
    normed = normed.astype(jnp.bfloat16).reshape(batch_rows, head_count * HD)
    attn_part = jnp.dot(normed, w_out, preferred_element_type=jnp.float32)
    attn_share = lax.psum_scatter(attn_part, "tp", scatter_dimension=1, tiled=True)
    residual = (tokens.astype(jnp.float32) + attn_share).astype(jnp.bfloat16)
    mlp_block, mlp_squares = spread_rows(residual, mlp_gain)
    gate_part = jnp.dot(mlp_block, w_gate, preferred_element_type=jnp.float32)
    up_part = jnp.dot(mlp_block, w_up, preferred_element_type=jnp.float32)
    gate_sum, up_sum = lax.psum((gate_part, up_part), "kv")
    second_rms = lax.rsqrt(mlp_squares / full_width + epsilon)[:, None]
    hidden = (jax.nn.silu(gate_sum * second_rms) * (up_sum * second_rms)).astype(jnp.bfloat16)
    down_part = jnp.dot(hidden, w_down, preferred_element_type=jnp.float32)
    mlp_share = lax.psum_scatter(down_part, "tp", scatter_dimension=1, tiled=True)
    return (residual.astype(jnp.float32) + mlp_share).astype(jnp.bfloat16)


def solution(mesh):
    placed = (
        P(None, ("kv", "tp")),
        P(),
        P(("kv", "tp")),
        P("kv", "tp"),
        P("kv", None),
        P("kv", None),
        P(),
        P(),
        P(None, None, ("kv", "tp")),
        P(None, None, ("kv", "tp")),
        P(None, None, ("kv", "tp")),
        P(),
        P("tp", "kv"),
        P(("kv", "tp")),
        P("kv", "tp"),
        P("kv", "tp"),
        P("tp", "kv"),
    )
    return jax.shard_map(
        body, mesh=mesh, in_specs=placed, out_specs=P(None, ("kv", "tp")), check_vma=False
    )
```

profile of v0, /device:TPU:0, one launch (start us, length us, event | category | flops | bytes accessed | tf_op | source)
XLA Modules:
  0.0 321.7 jit_solution(4829693310829404246)
XLA Ops:
  6.5 0.0 copy-start
  6.5 0.0 copy-start.2
  6.5 0.0 reduce-scatter.9.cloned.1.call-start
  6.5 0.9 dynamic_slice.19
  7.5 0.7 mul.150
  8.2 0.8 fusion.11
  8.9 42.0 %psum.71 = f32[3]{0:T(128)S(1)} all-reduce(f32[3]{0:T(128)S(1)} %get-tuple-element.23), channel_id=1, replica_groups=mesh['kv'=4,'tp'=8] {'kv','tp'}, use_global_device_ids=true, to_apply=%region_2.0 | all-reduce | flops 3 | bytes 24 | tf_op jit(solution)/shard_map/psum | solution.py:19
  50.9 0.0 copy-start.5
  51.0 10.6 %all_gather.9 = bf16[3,1024]{1,0:T(4,128)(2,1)S(1)} all-gather(bf16[3,128]{1,0:T(4,128)(2,1)S(1)} %get-tuple-element.24), channel_id=1, replica_groups=mesh['kv'=4,'tp'=8] {'tp'}, dimensions={1}, use_global_device_ids=true | all-gather | bytes 6912 | tf_op jit(solution)/shard_map/all_gather | solution.py:18
  61.5 1.7 fusion.25
  63.2 1.1 fusion.22
  64.3 1.2 fusion.21
  65.5 1.0 fusion.3
  66.5 9.9 %all-reduce.5 = (f32[3,256]{1,0:T(4,128)S(1)}, f32[3,32]{1,0:T(4,128)S(1)}, f32[3,128]{1,0:T(4,128)S(1)}) all-reduce(f32[3,256]{1,0:T(4,128)S(1)} %fusion.21, f32[3,32]{1,0:T(4,128)S(1)} %fusion.3, f32[3,128]{1,0:T(4,128)S(1)} %fusion.22), channel_id=1, replica_groups=mesh['kv'=4,'tp'=8] {'kv'}, use_global_device_ids=true, to_apply=%region_0.0 | all-reduce | flops 1248 | bytes 9984 | tf_op jit(solution)/shard_map/psum | solution.py:52
  76.4 0.1 multiply_convert_fusion.1
  76.5 0.1 multiply_convert_fusion.3
  76.5 0.1 reshape.90
  76.6 12.8 %all_gather.10 = bf16[3,2048]{1,0:T(4,128)(2,1)S(1)} all-gather(bf16[3,256]{1,0:T(4,128)(2,1)S(1)} %multiply_convert_fusion.1), channel_id=1, replica_groups=mesh['kv'=4,'tp'=8] {'tp'}, dimensions={1}, use_global_device_ids=true | all-gather | bytes 13824 | tf_op jit(solution)/shard_map/all_gather | solution.py:60
  89.4 0.1 reshape.78
  89.5 0.1 fusion.23
  89.6 0.1 mul.142
  89.7 0.0 copy-start.3
  89.7 1.1 convolution_multiply_fusion
  90.8 0.7 broadcast_compare_fusion
  91.5 0.0 copy-start.4
  91.5 0.0 copy-done.5
  91.5 0.7 fusion.16
  92.2 1.0 fusion
  93.2 0.0 copy-done.4
  93.2 0.1 select_reduce_fusion
  93.4 0.0 copy-done.3
  93.4 37.8 %pmax.7 = f32[3,32]{1,0:T(4,128)} all-reduce(f32[3,32]{1,0:T(4,128)S(1)} %max.17), channel_id=1, replica_groups=mesh['kv'=4,'tp'=8] {'kv','tp'}, use_global_device_ids=true, to_apply=%region_6.7 | all-reduce | flops 96 | bytes 768 | tf_op jit(solution)/shard_map/pmax | solution.py:87
  131.2 1.4 fusion.1
  132.6 1.2 dynamic-slice
  134.5 1.1 fusion.24
  135.6 27.4 %all-reduce.2 = (f32[3,32,64]{2,1,0:T(8,128)S(1)}, f32[3,32]{1,0:T(4,128)S(1)}) all-reduce(f32[3,32,64]{2,1,0:T(8,128)S(1)} %bitcast.42, f32[3,32]{1,0:T(4,128)} %get-tuple-element.21), channel_id=2, replica_groups=mesh['kv'=4,'tp'=8] {'tp'}, use_global_device_ids=true, to_apply=%region_7.8.clone | all-reduce | flops 6240 | bytes 49920
  163.0 0.1 constant_dynamic-slice_fusion
  163.1 16.6 %all-reduce.4 = (f32[3,4,64]{2,1,0:T(4,128)S(1)}, f32[3,4]{1,0:T(4,128)S(1)}, f32[3,128]{1,0:T(4,128)S(1)}) all-reduce(f32[3,4,64]{2,1,0:T(4,128)S(1)} %constant_dynamic-slice_fusion.1, f32[3,4]{1,0:T(4,128)S(1)} %constant_dynamic-slice_fusion, f32[3,128]{1,0:T(4,128)} %fusion.25), channel_id=1, replica_groups=mesh['kv'=4,'tp'=8] {'kv'}, use_global_device_ids=true, to_apply=%region_8.9 | all-reduce | flops 1164 | bytes 9312 | tf_op jit(solution)/shard_map/psum | solution.py:99
  179.7 0.7 multiply_convert_fusion.2
  180.4 0.1 reshape.84
  180.5 0.8 fusion.20
  181.2 0.2 multiply_reduce_fusion
  181.4 0.8 multiply_convert_fusion
  182.2 0.1 reshape.86
  182.2 0.0 copy-done.2
  182.3 1.1 convolution_bitcast_fusion.1
  183.4 0.0 reduce-scatter.9.cloned.1.call-update
  183.4 0.0 reduce-scatter.11.cloned.1.call-start
  183.5 27.8 %reduce-scatter.9.cloned.1.call-done = f32[128,3]{1,0:T(8,128)} async-done(((f32[1024,3]{1,0:T(8,128)}), f32[128,3]{1,0:T(8,128)}) %reduce-scatter.9.cloned.1.call-update) | async-done | bytes 1552
  211.3 0.9 copy.24
  212.2 0.8 fusion.14
  213.0 37.8 %psum.78 = f32[3]{0:T(128)S(1)} all-reduce(f32[3]{0:T(128)S(1)} %get-tuple-element.15), channel_id=1, replica_groups=mesh['kv'=4,'tp'=8] {'kv','tp'}, use_global_device_ids=true, to_apply=%region_17.18 | all-reduce | flops 3 | bytes 24 | tf_op jit(solution)/shard_map/psum | solution.py:19
  250.8 0.8 fusion.13
  251.6 11.4 %all_gather.11 = bf16[3,1024]{1,0:T(4,128)(2,1)S(1)} all-gather(bf16[3,128]{1,0:T(4,128)(2,1)S(1)} %fusion.13), channel_id=1, replica_groups=mesh['kv'=4,'tp'=8] {'tp'}, dimensions={1}, use_global_device_ids=true | all-gather | bytes 6912 | tf_op jit(solution)/shard_map/all_gather | solution.py:18
  263.0 0.0 copy-done
  263.0 0.5 fusion.27
  263.5 0.0 copy-done.1
  263.5 0.5 fusion.26
  264.0 16.7 %all-reduce.3 = (f32[3,1408]{1,0:T(4,128)S(1)}, f32[3,1408]{1,0:T(4,128)S(1)}) all-reduce(f32[3,1408]{1,0:T(4,128)S(1)} %fusion.27, f32[3,1408]{1,0:T(4,128)S(1)} %fusion.26), channel_id=1, replica_groups=mesh['kv'=4,'tp'=8] {'kv'}, use_global_device_ids=true, to_apply=%region_18.19 | all-reduce | flops 8448 | bytes 67584 | tf_op jit(solution)/shard_map/psum | solution.py:123
  280.7 3.8 %convolution_bitcast_fusion = f32[1024,3]{1,0:T(8,128)} fusion(bf16[1408,1024]{1,0:T(8,128)(2,1)} %param.33, f32[3,1408]{1,0:T(4,128)S(1)} %get-tuple-element.7, f32[3,1408]{1,0:T(4,128)S(1)} %get-tuple-element.8, f32[3]{0:T(128)S(1)} %add_rsqrt_fusion.1), kind=kOutput, calls=%fused_computation | convolution fusion | flops 8684544 | bytes 2929676
  284.5 0.0 reduce-scatter.11.cloned.1.call-update
  284.5 28.8 %reduce-scatter.11.cloned.1.call-done = f32[128,3]{1,0:T(8,128)} async-done(((f32[1024,3]{1,0:T(8,128)}), f32[128,3]{1,0:T(8,128)}) %reduce-scatter.11.cloned.1.call-update) | async-done | bytes 1552
  313.3 0.9 copy.26
  314.2 0.6 fusion.15
  (9 shorter events, 0.1 us)
Async XLA Ops:
  6.5 256.5 %copy-start = (bf16[1024,1408]{1,0:T(8,128)(2,1)S(1)}, bf16[1024,1408]{1,0:T(8,128)(2,1)}, u32[]{:S(2)}) copy-start(bf16[1024,1408]{1,0:T(8,128)(2,1)} %param.32) | copy-start | bytes 8650756
  6.5 175.7 %copy-start.2 = (bf16[256,1024]{1,0:T(8,128)(2,1)S(1)}, bf16[256,1024]{1,0:T(8,128)(2,1)}, u32[]{:S(2)}) copy-start(bf16[256,1024]{1,0:T(8,128)(2,1)} %param.29) | copy-start | bytes 1572868
  6.5 204.8 %reduce-scatter.9.cloned.1.call-start = ((), (), s32[]{:S(2)}) async-start(), calls=%async_computation.2 | async-start | bytes 589824
  50.9 40.6 %copy-start.5 = (f32[3]{0:T(128)}, f32[3]{0:T(128)S(1)}, u32[]{:S(2)}) copy-start(f32[3]{0:T(128)S(1)} %add_rsqrt_fusion.2) | copy-start | bytes 40
  89.7 3.7 %copy-start.3 = (f32[3,32]{1,0:T(4,128)}, f32[3,32]{1,0:T(4,128)S(1)}, u32[]{:S(2)}) copy-start(f32[3,32]{1,0:T(4,128)S(1)} %mul.142) | copy-start | bytes 1156
  91.5 1.7 copy-start.4
  183.4 129.9 %reduce-scatter.11.cloned.1.call-start = ((), (), s32[]{:S(2)}) async-start(), calls=%async_computation.3 | async-start | bytes 589824
  250.8 12.7 %copy-start.1 = (bf16[1024,1408]{1,0:T(8,128)(2,1)S(1)}, bf16[1024,1408]{1,0:T(8,128)(2,1)}, u32[]{:S(2)}) copy-start(bf16[1024,1408]{1,0:T(8,128)(2,1)} %param.31) | copy-start | bytes 8650756
Sparse Core Ops, SparseCore 0:
  183.5 27.7 reduce-scatter.8
  284.6 28.6 reduce-scatter.10
where the time goes:
time: 323 us; the launch traced here: 322 us
  blocking collectives  223 us (69%)
  waiting for transfers between devices  56.7 us (18%)
  between operations  14.1 us (4%)
  matrix products  13.2 us (4%)
  other arithmetic  9.52 us (3%)
  local copies, waits for them, and re-layouts  5.19 us (2%)
    psum x2, blocking collectives, spread_rows(): square_total = lax.psum(squares, ('kv', 'tp'))  79.8 us
    unnamed x4, waiting for transfers between devices  56.7 us
    pmax x1, blocking collectives, body(): score_top = lax.pmax(local_top, ('kv', 'tp'))  37.8 us
    unnamed x1, blocking collectives  27.4 us
    all_gather x2, blocking collectives, spread_rows(): row_block = lax.all_gather(scaled, 'tp', axis=1, tiled=True)  22 us
    psum x1, blocking collectives, body(): gate_sum, up_sum = lax.psum((gate_part, up_part), 'kv')  16.7 us
    psum x1, blocking collectives, body(): weight_total, value_sums = lax.psum((weight_total, value_sums), 'kv')  16.6 us
    all_gather x1, blocking collectives, body(): query_all = lax.all_gather(query_local, 'tp', axis=1, tiled=True)  12.8 us
  transfers between devices with their start and end apart: 2, of which 2 were waited for; matrix products, arithmetic and copies ran while one was open for 0% of the time, Pallas kernels for 0%

commit v1 on v0

--- a/solution.py
+++ b/solution.py
@@ -1,6 +1,10 @@
+import functools
+
 import jax
 import jax.numpy as jnp
 from jax import lax
+from jax.experimental import pallas as pl
+from jax.experimental.pallas import tpu as pltpu
 from jax.sharding import PartitionSpec as P
 
 QUERY_HEAD_COUNT = 32
@@ -128,6 +132,462 @@
     return (residual.astype(jnp.float32) + mlp_share).astype(jnp.bfloat16)
 
 
+LANES = 128
+ROWS = 8
+MESH = pl.DeviceIdType.MESH
+
+
+def column_chunks(columns):
+    first = (columns // LANES + 1) // 2 * LANES
+    return ((0, first), (first, columns))
+
+
+def exchange(buffer, mine, axis, count, send_sems, recv_sems, source=None):
+    copies = []
+    for step in range(1, count):
+        partner = lax.rem(mine + step, count)
+        copy = pltpu.make_async_remote_copy(
+            src_ref=buffer.at[mine] if source is None else source(partner),
+            dst_ref=buffer.at[mine],
+            send_sem=send_sems.at[step - 1],
+            recv_sem=recv_sems.at[step - 1],
+            device_id={axis: partner},
+            device_id_type=MESH,
+        )
+        copy.start()
+        copies.append(copy)
+    return copies
+
+
+def arrive(copies):
+    for copy in copies:
+        copy.wait_recv()
+
+
+def merge_partials(buffer, count, lane):
+    parts = [buffer[i] for i in range(count)]
+    tops = [part[:, HD : HD + 1] for part in parts]
+    top = functools.reduce(jnp.maximum, tops)
+    total = functools.reduce(
+        jnp.add, [jnp.exp(one - top) * part for one, part in zip(tops, parts)]
+    )
+    return jnp.where((lane >= HD) & (lane < HD + HD // 2), top, total)
+
+
+def layer_kernel(
+    kv_count,
+    tp_count,
+    lengths,
+    tokens,
+    attn_gain,
+    mlp_gain,
+    forget_bias,
+    out_gain,
+    w_query_hbm,
+    w_key_hbm,
+    w_value_hbm,
+    w_forget_hbm,
+    keys_hbm,
+    values_hbm,
+    decay_hbm,
+    w_out_hbm,
+    w_gate_hbm,
+    w_up_hbm,
+    w_down_hbm,
+    out,
+    w_query,
+    w_key,
+    w_value,
+    w_forget,
+    keys,
+    values,
+    decay,
+    w_out,
+    w_gate,
+    w_up,
+    w_down,
+    token_buf,
+    proj_buf,
+    query_buf,
+    part_send,
+    part_buf,
+    merged_buf,
+    normed_buf,
+    attn_buf,
+    residual_buf,
+    square_buf,
+    gate_buf0,
+    gate_buf1,
+    down_send,
+    down_buf,
+    local_sem,
+    tp_send,
+    tp_recv,
+    kv_send,
+    kv_recv,
+):
+    kv = lax.axis_index("kv")
+    tp = lax.axis_index("tp")
+    batch = tokens.shape[0]
+    half = ROWS // 2
+    width = tokens.shape[1] * kv_count * tp_count
+    block = w_query.shape[0]
+    span = keys.shape[2]
+    f32, bf16 = jnp.float32, jnp.bfloat16
+
+    loads = {}
+
+    def load(name, source, target):
+        copy = pltpu.make_async_copy(source, target, local_sem.at[len(loads)])
+        copy.start()
+        loads[name] = copy
+
+    load("query", w_query_hbm, w_query)
+    load("key", w_key_hbm, w_key)
+    load("value", w_value_hbm, w_value)
+    load("forget", w_forget_hbm.at[pl.ds(pl.multiple_of(kv * block, block), block), :], w_forget)
+
+    barrier = pltpu.get_barrier_semaphore()
+    for step in range(1, tp_count):
+        pl.semaphore_signal(
+            barrier, inc=1, device_id={"tp": lax.rem(tp + step, tp_count)}, device_id_type=MESH
+        )
+    for step in range(1, kv_count):
+        pl.semaphore_signal(
+            barrier, inc=1, device_id={"kv": lax.rem(kv + step, kv_count)}, device_id_type=MESH
+        )
+    token_buf[tp, 0:batch, :] = tokens[...].astype(f32)
+    token_buf[tp, batch : batch + 1, :] = attn_gain[...]
+    token_buf[tp, batch + 1 : batch + 2, :] = mlp_gain[...]
+    token_buf[tp, batch + 2 : ROWS, :] = jnp.zeros((ROWS - batch - 2, LANES), f32)
+    pl.semaphore_wait(barrier, tp_count + kv_count - 2)
+
+    pending = []
+
+    def tp_exchange(index, buffer, source=None):
+        copies = exchange(
+            buffer, tp, "tp", tp_count, tp_send.at[index], tp_recv.at[index], source
+        )
+        pending.extend(copies)
+        return copies
+
+    def kv_exchange(index, buffer):
+        copies = exchange(buffer, kv, "kv", kv_count, kv_send.at[index], kv_recv.at[index])
+        pending.extend(copies)
+        return copies
+
+    token_copies = tp_exchange(0, token_buf)
+    load("keys", keys_hbm, keys)
+    for c in range(span // LANES):
+        load("decay%d" % c, decay_hbm.at[:, :, pl.ds(c * LANES, LANES)], decay.at[c])
+    load("values", values_hbm, values)
+    load("out", w_out_hbm, w_out)
+    load("gate", w_gate_hbm, w_gate)
+    load("up", w_up_hbm, w_up)
+    load("down", w_down_hbm, w_down)
+    part_send[...] = jnp.zeros(part_send.shape, f32)
+    down_send[...] = jnp.zeros(down_send.shape, f32)
+
+    arrive(token_copies)
+    blocks = [token_buf[i] for i in range(tp_count)]
+    scaled = jnp.concatenate([b * b[batch : batch + 1, :] for b in blocks], axis=1).astype(bf16)
+    squares = functools.reduce(jnp.add, [b * b for b in blocks])
+    squares = jnp.sum(squares, axis=1, keepdims=True)
+    loads["query"].wait()
+    query = jnp.dot(scaled, w_query[...], preferred_element_type=f32)
+    loads["key"].wait()
+    key = jnp.dot(scaled, w_key[...], preferred_element_type=f32)
+    loads["value"].wait()
+    value = jnp.dot(scaled, w_value[...], preferred_element_type=f32)
+    loads["forget"].wait()
+    forget = jnp.dot(scaled, w_forget[...], preferred_element_type=f32)
+    proj_buf[kv, 0] = jnp.concatenate([query[:half, :LANES], query[:half, LANES:]], axis=0)
+    proj_buf[kv, 1] = jnp.concatenate([key[:half], value[:half]], axis=0)
+    heads = forget.shape[1]
+    proj_buf[kv, 2, :, 0:heads] = forget
+    proj_buf[kv, 2, :, heads:LANES] = jnp.broadcast_to(squares, (ROWS, LANES - heads))
+    arrive(kv_exchange(0, proj_buf))
+    sums = [
+        functools.reduce(jnp.add, [proj_buf[i, piece] for i in range(kv_count)])
+        for piece in range(3)
+    ]
+    rms = lax.rsqrt(sums[2][:, heads : heads + 1] / width + epsilon)
+    rms_twice = jnp.concatenate([rms[:half], rms[:half]], axis=0)
+    query_rows = pl.ds(pl.multiple_of(tp * ROWS, ROWS), ROWS)
+    query_buf[tp] = (sums[0] * rms_twice).astype(bf16).astype(f32)
+    query_copies = tp_exchange(1, query_buf)
+    new_rows = (sums[1] * rms_twice).astype(bf16).astype(f32)
+    raw_gate = sums[2][:, 0:heads] * rms + forget_bias[...]
+    log_gate = jnp.minimum(raw_gate, 0.0) - jnp.log1p(jnp.exp(-jnp.abs(raw_gate)))
+
+    lane = lax.broadcasted_iota(jnp.int32, (ROWS, LANES), 1)
+    group_rows = heads // KV_HEADS
+    row_id = lax.broadcasted_iota(jnp.int32, (heads, heads), 0)
+    row_rest = row_id % group_rows
+    head_of_row = (
+        row_id // group_rows * group_rows + row_rest % (group_rows // 2) * 2
+        + row_rest // (group_rows // 2)
+    )
+    head_pick = head_of_row == lax.broadcasted_iota(jnp.int32, (heads, heads), 1)
+    slots = lax.broadcasted_iota(jnp.int32, (heads, span), 1)
+    slots = slots + (kv * tp_count + tp) * span
+    first_device = jnp.broadcast_to(kv * tp_count + tp, (heads, 1)) == 0
+    score_scale = HD ** (-0.5)
+    arrive(query_copies)
+    query_flat = query_buf.reshape(tp_count * ROWS, LANES)
+    half_rows = group_rows // 2
+    pairs = [(g, p) for g in range(KV_HEADS) for p in range(2)]
+    loads["keys"].wait()
+    loads["values"].wait()
+    for c in range(span // LANES):
+        loads["decay%d" % c].wait()
+    for b in range(batch):
+        pieces = []
+        for g, p in pairs:
+            rows = query_flat[pl.ds(g * half_rows * half + b, half_rows, stride=half), :]
+            if p != g:
+                rows = pltpu.roll(rows, HD, 1)
+            pieces.append(jnp.where(lane // HD == g, rows, 0.0))
+        queries = jnp.concatenate(pieces, axis=0)
+        own = jnp.sum(queries * new_rows[b : b + 1, :], axis=1, keepdims=True) * score_scale
+        scores = jnp.dot(queries.astype(bf16), keys[b], preferred_element_type=f32)
+        faded = jnp.concatenate(
+            [
+                jnp.concatenate(
+                    [
+                        decay[c, b, pl.ds(g * group_rows + p, half_rows, stride=2), :]
+                        for g, p in pairs
+                    ],
+                    axis=0,
+                )
+                for c in range(span // LANES)
+            ],
+            axis=1,
+        )
+        gate_rows = jnp.sum(
+            jnp.where(head_pick, log_gate[b : b + 1, :], 0.0), axis=1, keepdims=True
+        )
+        live = slots < lengths[b]
+        scores = jnp.where(live, scores * score_scale + faded + gate_rows, masked_score)
+        top = jnp.max(scores, axis=1, keepdims=True)
+        top = jnp.where(first_device, jnp.maximum(top, own), top)
+        weights = jnp.where(live, jnp.exp(scores - top), 0.0)
+        own_weight = jnp.where(first_device, jnp.exp(jnp.minimum(own - top, 0.0)), 0.0)
+        total = jnp.sum(weights, axis=1, keepdims=True) + own_weight
+        mixed = lax.dot_general(
+            weights.astype(bf16),
+            values[b],
+            (((1,), (1,)), ((), ())),
+            preferred_element_type=f32,
+        )
+        mixed = mixed + own_weight * new_rows[half + b : half + b + 1, :]
+        for i, (g, p) in enumerate(pairs):
+            rows = slice(i * half_rows, (i + 1) * half_rows)
+            tile = mixed[rows]
+            if g:
+                tile = pltpu.roll(tile, HD, 1)
+            tile = jnp.where(
+                lane < HD, tile, jnp.where(lane < HD + HD // 2, top[rows], total[rows])
+            )
+            part_send[pl.ds(g * half_rows * ROWS + 2 * b + p, half_rows, stride=ROWS), :] = tile
+
+    def part_of(index):
+        return pl.ds(pl.multiple_of(index * 2 * ROWS, 2 * ROWS), 2 * ROWS)
+
+    part_copies = tp_exchange(2, part_buf, lambda partner: part_send.at[part_of(partner), :])
+    part_buf[tp] = part_send[part_of(tp), :]
+    lane2 = lax.broadcasted_iota(jnp.int32, (2 * ROWS, LANES), 1)
+    row2 = lax.broadcasted_iota(jnp.int32, (2 * ROWS, LANES), 0)
+    gain_row = lax.broadcasted_iota(jnp.int32, out_gain.shape, 0)
+    gain_tiles = []
+    for j in range(2):
+        gain = jnp.sum(
+            jnp.where(gain_row == 2 * tp + j, out_gain[...], 0.0), axis=0, keepdims=True
+        )
+        gain = jnp.broadcast_to(gain, (ROWS, LANES))
+        gain_tiles.append(jnp.where(row2[:ROWS] % 2 == 0, gain, pltpu.roll(gain, HD, 1)))
+    gains = jnp.concatenate(gain_tiles, axis=0)
+    arrive(part_copies)
+    merged_buf[kv] = merge_partials(part_buf, tp_count, lane2)
+    arrive(kv_exchange(1, merged_buf))
+    merged = merge_partials(merged_buf, kv_count, lane2)
+    total = merged[:, HD + HD // 2 : HD + HD // 2 + 1]
+    total = jnp.where(row2[:, 0:1] % ROWS < 2 * batch, total, 1.0)
+    heads_out = jnp.where(lane2 < HD, merged / total, 0.0)
+    mean = jnp.sum(heads_out * heads_out, axis=1, keepdims=True) / HD
+    normed_buf[...] = heads_out * lax.rsqrt(mean + epsilon) * gains
+    columns = []
+    for j in range(2):
+        even = normed_buf[pl.ds(j * ROWS, half, stride=2), :]
+        odd = normed_buf[pl.ds(j * ROWS + 1, half, stride=2), :]
+        columns.append(jnp.where(lane[:half] < HD, even, pltpu.roll(odd, HD, 1)))
+    normed = jnp.concatenate(columns, axis=1).astype(bf16)
+
+    loads["out"].wait()
+    attn = jnp.dot(normed, w_out[...], preferred_element_type=f32)
+    middle = attn.shape[1] // 2
+    attn_buf[tp] = jnp.concatenate([attn[:, :middle], attn[:, middle:]], axis=0).astype(bf16)
+    arrive(tp_exchange(3, attn_buf))
+    attn = functools.reduce(jnp.add, [attn_buf[i].astype(f32) for i in range(tp_count)])
+    attn = jnp.concatenate([attn[:half], attn[half:]], axis=1)
+    token_rows = jnp.concatenate([token_buf[i][:half] for i in range(tp_count)], axis=1)
+    residual = (token_rows + attn).astype(bf16).astype(f32)
+    squares = jnp.sum(residual * residual, axis=1, keepdims=True)
+    square_buf[kv] = jnp.broadcast_to(
+        jnp.concatenate([squares, squares], axis=0), (ROWS, LANES)
+    )
+    square_copies = kv_exchange(2, square_buf)
+    for i in range(tp_count):
+        residual_buf[i, 0:half, :] = residual[:, i * LANES : (i + 1) * LANES]
+    gain_rows = jnp.concatenate(
+        [token_buf[i][batch + 1 : batch + 2] for i in range(tp_count)], axis=1
+    )
+    scaled = (residual * gain_rows).astype(bf16)
+
+    loads["gate"].wait()
+    loads["up"].wait()
+    chunks = column_chunks(w_gate.shape[1])
+    gate_bufs = (gate_buf0, gate_buf1)
+    gate_copies = []
+    for index, (begin, end) in enumerate(chunks):
+        gate = jnp.dot(scaled, w_gate[:, begin:end], preferred_element_type=f32)
+        up = jnp.dot(scaled, w_up[:, begin:end], preferred_element_type=f32)
+        gate_bufs[index][kv] = jnp.concatenate([gate, up], axis=0).astype(bf16)
+        gate_copies.append(kv_exchange(3 + index, gate_bufs[index]))
+    arrive(square_copies)
+    squares = functools.reduce(jnp.add, [square_buf[i] for i in range(kv_count)])
+    rms = lax.rsqrt(squares[:half, 0:1] / width + epsilon)
+    loads["down"].wait()
+    down = jnp.zeros((half, w_down.shape[1]), f32)
+    for index, (begin, end) in enumerate(chunks):
+        arrive(gate_copies[index])
+        both = functools.reduce(
+            jnp.add, [gate_bufs[index][i].astype(f32) for i in range(kv_count)]
+        )
+        gate, up = both[:half] * rms, both[half:] * rms
+        hidden = (gate / (1.0 + jnp.exp(-gate)) * up).astype(bf16)
+        down = down + jnp.dot(hidden, w_down[begin:end, :], preferred_element_type=f32)
+    for i in range(tp_count):
+        down_send[i, 0:half, :] = down[:, i * LANES : (i + 1) * LANES]
+    down_copies = tp_exchange(4, down_buf, lambda partner: down_send.at[partner])
+    down_buf[tp] = down_send[tp]
+    arrive(down_copies)
+    share = functools.reduce(jnp.add, [down_buf[i] for i in range(tp_count)])
+    final = residual_buf[tp][0:batch] + share[0:batch]
+    out[...] = final.astype(bf16)
+    for copy in pending:
+        copy.wait_send()
+
+
+def kernel_layer(
+    kv_count,
+    tp_count,
+    tokens,
+    lengths,
+    attn_gain,
+    w_query,
+    w_key,
+    w_value,
+    w_forget,
+    forget_bias,
+    cache_keys,
+    cache_values,
+    cache_decay,
+    out_gain,
+    w_out,
+    mlp_gain,
+    w_gate,
+    w_up,
+    w_down,
+):
+    f32, bf16 = jnp.float32, jnp.bfloat16
+    batch, _, span = cache_keys.shape
+    heads = w_forget.shape[1]
+    block = w_query.shape[0]
+    columns = w_out.shape[1]
+    chunks = column_chunks(w_gate.shape[1])
+    in_vmem = pl.BlockSpec(memory_space=pltpu.VMEM)
+    anywhere = pl.BlockSpec(memory_space=pl.ANY)
+    chunk_count = span // LANES
+    dma = pltpu.SemaphoreType.DMA
+    scratch = [
+        pltpu.VMEM(w_query.shape, bf16),
+        pltpu.VMEM(w_key.shape, bf16),
+        pltpu.VMEM(w_value.shape, bf16),
+        pltpu.VMEM((block, heads), bf16),
+        pltpu.VMEM(cache_keys.shape, bf16),
+        pltpu.VMEM(cache_values.shape, bf16),
+        pltpu.VMEM((chunk_count, batch, heads, LANES), f32),
+        pltpu.VMEM(w_out.shape, bf16),
+        pltpu.VMEM(w_gate.shape, bf16),
+        pltpu.VMEM(w_up.shape, bf16),
+        pltpu.VMEM(w_down.shape, bf16),
+        pltpu.VMEM((tp_count, ROWS, LANES), f32),
+        pltpu.VMEM((kv_count, 3, ROWS, LANES), f32),
+        pltpu.VMEM((tp_count, ROWS, LANES), f32),
+        pltpu.VMEM((tp_count * 2 * ROWS, LANES), f32),
+        pltpu.VMEM((tp_count, 2 * ROWS, LANES), f32),
+        pltpu.VMEM((kv_count, 2 * ROWS, LANES), f32),
+        pltpu.VMEM((2 * ROWS, LANES), f32),
+        pltpu.VMEM((tp_count, ROWS, columns // 2), bf16),
+        pltpu.VMEM((tp_count, ROWS, LANES), f32),
+        pltpu.VMEM((kv_count, ROWS, LANES), f32),
+        pltpu.VMEM((kv_count, ROWS, chunks[0][1] - chunks[0][0]), bf16),
+        pltpu.VMEM((kv_count, ROWS, chunks[1][1] - chunks[1][0]), bf16),
+        pltpu.VMEM((tp_count, ROWS, LANES), f32),
+        pltpu.VMEM((tp_count, ROWS, LANES), f32),
+        dma((10 + chunk_count,)),
+        dma((5, tp_count - 1)),
+        dma((5, tp_count - 1)),
+        dma((5, kv_count - 1)),
+        dma((5, kv_count - 1)),
+    ]
+    return pl.pallas_call(
+        functools.partial(layer_kernel, kv_count, tp_count),
+        out_shape=jax.ShapeDtypeStruct(tokens.shape, bf16),
+        in_specs=[pl.BlockSpec(memory_space=pltpu.SMEM)] + [in_vmem] * 5 + [anywhere] * 11,
+        out_specs=in_vmem,
+        scratch_shapes=scratch,
+        compiler_params=pltpu.CompilerParams(
+            collective_id=0, has_side_effects=True, vmem_limit_bytes=60 * 1024 * 1024
+        ),
+        name="decode_layer",
+    )(
+        lengths,
+        tokens,
+        attn_gain.reshape(1, -1),
+        mlp_gain.reshape(1, -1),
+        forget_bias.reshape(1, -1),
+        out_gain.reshape(-1, LANES),
+        w_query,
+        w_key,
+        w_value,
+        w_forget,
+        cache_keys,
+        cache_values,
+        cache_decay,
+        w_out,
+        w_gate,
+        w_up,
+        w_down,
+    )
+
+
+def dispatch(kv_count, tp_count, *arrays):
+    tokens, w_query, cache_keys, w_gate = arrays[0], arrays[3], arrays[8], arrays[14]
+    fits = (
+        tokens.shape[0] <= 3
+        and tokens.shape[1] == LANES
+        and w_query.shape[1] == 4 * HD
+        and tp_count == ROWS
+        and cache_keys.shape[2] % LANES == 0
+        and w_gate.shape[1] % LANES == 0
+    )
+    if fits:
+        return kernel_layer(kv_count, tp_count, *arrays)
+    return body(*arrays)
+
+
 def solution(mesh):
     placed = (
         P(None, ("kv", "tp")),
@@ -148,6 +608,7 @@
         P("kv", "tp"),
         P("tp", "kv"),
     )
+    chosen = functools.partial(dispatch, mesh.shape["kv"], mesh.shape["tp"])
     return jax.shard_map(
-        body, mesh=mesh, in_specs=placed, out_specs=P(None, ("kv", "tp")), check_vma=False
-    )
+        chosen, mesh=mesh, in_specs=placed, out_specs=P(None, ("kv", "tp")), check_vma=False
+    )

time: 323 us -> 43 us (0.13)
  blocking collectives: 223 us -> 0 us
  waiting for transfers between devices: 56.7 us -> 0 us
  Pallas kernels: 0 us -> 39.3 us
  between operations: 14.1 us -> 0.01 us
  matrix products: 13.2 us -> 0 us
  other arithmetic: 9.52 us -> 0 us
    psum x5 -> x0, blocking collectives: 123 us -> none  [the longest x2 79.8 us: spread_rows(): square_total = lax.psum(squares, ('kv', 'tp'))]
    unnamed x4 -> x0, waiting for transfers between devices: 56.7 us -> none
    pallas_call x0 -> x1, Pallas kernels: none -> 39.3 us  [kernel_layer(): pl.pallas_call(functools.partial(layer_kernel, kv_count, tp_count), out_s...]
    pmax x1 -> x0, blocking collectives: 37.8 us -> none  [body(): score_top = lax.pmax(local_top, ('kv', 'tp'))]
    all_gather x3 -> x0, blocking collectives: 34.7 us -> none  [the longest x2 22 us: spread_rows(): row_block = lax.all_gather(scaled, 'tp', axis=1, tiled=True)]
    unnamed x1 -> x0, blocking collectives: 27.4 us -> none
    dot_general x9 -> x0, matrix products: 8.21 us -> none  [the longest x1 1.67 us: body(): value_part = jnp.dot(row_block, w_value, preferred_element_type=jnp.float32)]
    unnamed x2 -> x0, matrix products: 4.98 us -> none
  transfers between devices with their start and end apart: 2 -> 0, of which waited for: 2 -> 0; matrix products, arithmetic and copies ran while one was open for 0% -> 0% of each run, Pallas kernels for 0% -> 0%
where the time goes in v1:
time: 43 us; the launch traced here: 42.8 us
  Pallas kernels  39.3 us (91%)
  local copies, waits for them, and re-layouts  3.52 us (8%)
    pallas_call x1, Pallas kernels, kernel_layer(): pl.pallas_call(functools.partial(layer_kernel, kv_count, tp_count), out_s...  39.3 us
    unnamed x2, local copies, waits for them, and re-layouts  3.52 us

profile of v1, /device:TPU:0, one launch (start us, length us, event | category | flops | bytes accessed | tf_op | source)
XLA Modules:
  0.0 42.8 jit_solution(17977205141046874124)
XLA Ops:
  0.0 2.3 %copy.18.w_forget_hbm = bf16[4096,32]{1,0:T(8,128)(2,1)} copy(bf16[4096,32]{0,1:T(8,128)(2,1)} %param.23) | data formatting | bytes 524288 | tf_op args[6]
  2.3 39.3 %decode_layer.1 = bf16[3,128]{1,0:T(4,128)(2,1)} custom-call(s32[3]{0:T(128)} %lengths.1, bf16[3,128]{1,0:T(4,128)(2,1)} %tokens.1, f32[1,128]{1,0:T(1,128)} %bitcast.5, f32[1,128]{1,0:T(1,128)} %bitcast.6, f32[1,32]{1,0:T(1,128)} %bitcast.7, f32[16,128]{1,0:T(8,128)} %bitcast.4, bf16[1024,256]{1,0:T(8,128)(2,1)} %w_query_hbm.1, ...), custom_call_target="tpu_custom_call" | custom-call | tf_op jit(solution)/shard_map/decode_layer/pallas_call | solution.py:545
  41.6 1.2 %copy.20 = bf16[3,128]{1,0:T(4,128)(2,1)} copy(bf16[3,128]{1,0:T(4,128)(2,1)} %decode_layer.1) | data formatting | bytes 1536

commit v2 on v1

--- a/solution.py
+++ b/solution.py
@@ -164,25 +164,39 @@
         copy.wait_recv()
 
 
+SLOT = HD // 4
+
+
+def tops_of(part):
+    starts = [HD + i * SLOT for i in range(3)]
+    return functools.reduce(jnp.add, [part[:, i : i + 1] for i in starts])
+
+
+def totals_of(part):
+    start = HD + 3 * SLOT
+    return part[:, start : start + 1] + part[:, start + SLOT // 2 : start + SLOT // 2 + 1]
+
+
 def merge_partials(buffer, count, lane):
-    parts = [buffer[i] for i in range(count)]
-    tops = [part[:, HD : HD + 1] for part in parts]
+    parts = [buffer[i].astype(jnp.float32) for i in range(count)]
+    tops = [tops_of(part) for part in parts]
     top = functools.reduce(jnp.maximum, tops)
     total = functools.reduce(
         jnp.add, [jnp.exp(one - top) * part for one, part in zip(tops, parts)]
     )
-    return jnp.where((lane >= HD) & (lane < HD + HD // 2), top, total)
+    total = jnp.where((lane >= HD) & (lane < HD + 3 * SLOT), 0.0, total)
+    return jnp.where((lane >= HD) & (lane < HD + SLOT), top, total)
 
 
 def layer_kernel(
     kv_count,
     tp_count,
-    lengths,
-    tokens,
-    attn_gain,
-    mlp_gain,
-    forget_bias,
-    out_gain,
+    lengths_hbm,
+    tokens_hbm,
+    attn_gain_hbm,
+    mlp_gain_hbm,
+    forget_bias_hbm,
+    out_gain_hbm,
     w_query_hbm,
     w_key_hbm,
     w_value_hbm,
@@ -195,6 +209,12 @@
     w_up_hbm,
     w_down_hbm,
     out,
+    lengths,
+    tokens,
+    attn_gain,
+    forget_bias,
+    out_gain,
+    stage,
     w_query,
     w_key,
     w_value,
@@ -207,8 +227,12 @@
     w_up,
     w_down,
     token_buf,
+    gain_buf,
     proj_buf,
+    new_buf,
+    query_wire,
     query_buf,
+    part_rows,
     part_send,
     part_buf,
     merged_buf,
@@ -242,11 +266,8 @@
         copy.start()
         loads[name] = copy
 
-    load("query", w_query_hbm, w_query)
-    load("key", w_key_hbm, w_key)
-    load("value", w_value_hbm, w_value)
-    load("forget", w_forget_hbm.at[pl.ds(pl.multiple_of(kv * block, block), block), :], w_forget)
-
+    load("tokens", tokens_hbm, tokens)
+    load("attn_gain", attn_gain_hbm, attn_gain)
     barrier = pltpu.get_barrier_semaphore()
     for step in range(1, tp_count):
         pl.semaphore_signal(
@@ -256,10 +277,21 @@
         pl.semaphore_signal(
             barrier, inc=1, device_id={"kv": lax.rem(kv + step, kv_count)}, device_id_type=MESH
         )
-    token_buf[tp, 0:batch, :] = tokens[...].astype(f32)
-    token_buf[tp, batch : batch + 1, :] = attn_gain[...]
-    token_buf[tp, batch + 1 : batch + 2, :] = mlp_gain[...]
-    token_buf[tp, batch + 2 : ROWS, :] = jnp.zeros((ROWS - batch - 2, LANES), f32)
+    stage[...] = jnp.zeros(stage.shape, f32)
+    load("mlp_gain", mlp_gain_hbm, gain_buf.at[tp])
+    load("query", w_query_hbm, w_query)
+    load("key", w_key_hbm, w_key)
+    load("value", w_value_hbm, w_value)
+    load("forget", w_forget_hbm.at[:, pl.ds(pl.multiple_of(kv * block, block), block)], w_forget)
+    load("forget_bias", forget_bias_hbm, forget_bias)
+    load("out_gain", out_gain_hbm, out_gain)
+    load("lengths", lengths_hbm, lengths)
+    loads["tokens"].wait()
+    loads["attn_gain"].wait()
+    own_tokens = tokens[...].astype(f32)
+    stage[0:batch, :] = own_tokens * attn_gain[...]
+    stage[half : half + batch, :] = own_tokens
+    token_buf[tp] = stage[...].astype(bf16)
     pl.semaphore_wait(barrier, tp_count + kv_count - 2)
 
     pending = []
@@ -285,39 +317,53 @@
     load("gate", w_gate_hbm, w_gate)
     load("up", w_up_hbm, w_up)
     load("down", w_down_hbm, w_down)
-    part_send[...] = jnp.zeros(part_send.shape, f32)
-    down_send[...] = jnp.zeros(down_send.shape, f32)
+    part_rows[...] = jnp.zeros(part_rows.shape, f32)
 
     arrive(token_copies)
     blocks = [token_buf[i] for i in range(tp_count)]
-    scaled = jnp.concatenate([b * b[batch : batch + 1, :] for b in blocks], axis=1).astype(bf16)
-    squares = functools.reduce(jnp.add, [b * b for b in blocks])
-    squares = jnp.sum(squares, axis=1, keepdims=True)
+    scaled = jnp.concatenate(blocks, axis=1)
+    token_rows = scaled.astype(f32)[half:]
+    squares = jnp.sum(token_rows * token_rows, axis=1, keepdims=True)
+    squares = jnp.concatenate([squares, squares], axis=0)
     loads["query"].wait()
     query = jnp.dot(scaled, w_query[...], preferred_element_type=f32)
+    proj_buf[kv, 0] = jnp.concatenate([query[:half, :LANES], query[:half, LANES:]], axis=0)
+    proj_buf[kv, 1] = jnp.broadcast_to(squares, (ROWS, LANES))
+    proj_copies = kv_exchange(0, proj_buf)
     loads["key"].wait()
     key = jnp.dot(scaled, w_key[...], preferred_element_type=f32)
     loads["value"].wait()
     value = jnp.dot(scaled, w_value[...], preferred_element_type=f32)
     loads["forget"].wait()
-    forget = jnp.dot(scaled, w_forget[...], preferred_element_type=f32)
-    proj_buf[kv, 0] = jnp.concatenate([query[:half, :LANES], query[:half, LANES:]], axis=0)
-    proj_buf[kv, 1] = jnp.concatenate([key[:half], value[:half]], axis=0)
+    forget = lax.dot_general(
+        scaled, w_forget[...], (((1,), (1,)), ((), ())), preferred_element_type=f32
+    )
+    new_buf[kv, 0] = jnp.concatenate([key[:half], value[:half]], axis=0)
     heads = forget.shape[1]
-    proj_buf[kv, 2, :, 0:heads] = forget
-    proj_buf[kv, 2, :, heads:LANES] = jnp.broadcast_to(squares, (ROWS, LANES - heads))
-    arrive(kv_exchange(0, proj_buf))
-    sums = [
+    new_buf[kv, 1, :, 0:heads] = forget
+    new_buf[kv, 1, :, heads:LANES] = jnp.zeros((ROWS, LANES - heads), f32)
+    new_copies = kv_exchange(5, new_buf)
+    loads["mlp_gain"].wait()
+    arrive(proj_copies)
+    query_sum, square_sum = [
         functools.reduce(jnp.add, [proj_buf[i, piece] for i in range(kv_count)])
-        for piece in range(3)
+        for piece in range(2)
     ]
-    rms = lax.rsqrt(sums[2][:, heads : heads + 1] / width + epsilon)
+    rms = lax.rsqrt(square_sum[:, 0:1] / width + epsilon)
     rms_twice = jnp.concatenate([rms[:half], rms[:half]], axis=0)
-    query_rows = pl.ds(pl.multiple_of(tp * ROWS, ROWS), ROWS)
-    query_buf[tp] = (sums[0] * rms_twice).astype(bf16).astype(f32)
-    query_copies = tp_exchange(1, query_buf)
-    new_rows = (sums[1] * rms_twice).astype(bf16).astype(f32)
-    raw_gate = sums[2][:, 0:heads] * rms + forget_bias[...]
+    query_wire[tp] = (query_sum * rms_twice).astype(bf16)
+    query_copies = tp_exchange(1, query_wire)
+    gain_copies = tp_exchange(5, gain_buf)
+    loads["forget_bias"].wait()
+    loads["out_gain"].wait()
+    loads["lengths"].wait()
+    arrive(new_copies)
+    new_sum, forget_sum = [
+        functools.reduce(jnp.add, [new_buf[i, piece] for i in range(kv_count)])
+        for piece in range(2)
+    ]
+    new_rows = (new_sum * rms_twice).astype(bf16).astype(f32)
+    raw_gate = forget_sum[:, 0:heads] * rms + forget_bias[...]
     log_gate = jnp.minimum(raw_gate, 0.0) - jnp.log1p(jnp.exp(-jnp.abs(raw_gate)))
 
     lane = lax.broadcasted_iota(jnp.int32, (ROWS, LANES), 1)
@@ -334,6 +380,7 @@
     first_device = jnp.broadcast_to(kv * tp_count + tp, (heads, 1)) == 0
     score_scale = HD ** (-0.5)
     arrive(query_copies)
+    query_buf[...] = query_wire[...].astype(f32)
     query_flat = query_buf.reshape(tp_count * ROWS, LANES)
     half_rows = group_rows // 2
     pairs = [(g, p) for g in range(KV_HEADS) for p in range(2)]
@@ -386,10 +433,17 @@
             tile = mixed[rows]
             if g:
                 tile = pltpu.roll(tile, HD, 1)
-            tile = jnp.where(
-                lane < HD, tile, jnp.where(lane < HD + HD // 2, top[rows], total[rows])
-            )
-            part_send[pl.ds(g * half_rows * ROWS + 2 * b + p, half_rows, stride=ROWS), :] = tile
+            rest = top[rows]
+            for start in range(HD, HD + 3 * SLOT, SLOT):
+                piece = rest.astype(bf16).astype(f32)
+                tile = jnp.where(lane < start, tile, piece)
+                rest = rest - piece
+            high = total[rows].astype(bf16).astype(f32)
+            tile = jnp.where(lane < HD + 3 * SLOT, tile, high)
+            tile = jnp.where(lane < HD + 3 * SLOT + SLOT // 2, tile, total[rows] - high)
+            part_rows[pl.ds(g * half_rows * ROWS + 2 * b + p, half_rows, stride=ROWS), :] = tile
+
+    part_send[...] = part_rows[...].astype(bf16)
 
     def part_of(index):
         return pl.ds(pl.multiple_of(index * 2 * ROWS, 2 * ROWS), 2 * ROWS)
@@ -411,7 +465,7 @@
     merged_buf[kv] = merge_partials(part_buf, tp_count, lane2)
     arrive(kv_exchange(1, merged_buf))
     merged = merge_partials(merged_buf, kv_count, lane2)
-    total = merged[:, HD + HD // 2 : HD + HD // 2 + 1]
+    total = totals_of(merged)
     total = jnp.where(row2[:, 0:1] % ROWS < 2 * batch, total, 1.0)
     heads_out = jnp.where(lane2 < HD, merged / total, 0.0)
     mean = jnp.sum(heads_out * heads_out, axis=1, keepdims=True) / HD
@@ -430,7 +484,6 @@
     arrive(tp_exchange(3, attn_buf))
     attn = functools.reduce(jnp.add, [attn_buf[i].astype(f32) for i in range(tp_count)])
     attn = jnp.concatenate([attn[:half], attn[half:]], axis=1)
-    token_rows = jnp.concatenate([token_buf[i][:half] for i in range(tp_count)], axis=1)
     residual = (token_rows + attn).astype(bf16).astype(f32)
     squares = jnp.sum(residual * residual, axis=1, keepdims=True)
     square_buf[kv] = jnp.broadcast_to(
@@ -439,9 +492,8 @@
     square_copies = kv_exchange(2, square_buf)
     for i in range(tp_count):
         residual_buf[i, 0:half, :] = residual[:, i * LANES : (i + 1) * LANES]
-    gain_rows = jnp.concatenate(
-        [token_buf[i][batch + 1 : batch + 2] for i in range(tp_count)], axis=1
-    )
+    arrive(gain_copies)
+    gain_rows = jnp.concatenate([gain_buf[i] for i in range(tp_count)], axis=1)
     scaled = (residual * gain_rows).astype(bf16)
 
     loads["gate"].wait()
@@ -468,7 +520,7 @@
         hidden = (gate / (1.0 + jnp.exp(-gate)) * up).astype(bf16)
         down = down + jnp.dot(hidden, w_down[begin:end, :], preferred_element_type=f32)
     for i in range(tp_count):
-        down_send[i, 0:half, :] = down[:, i * LANES : (i + 1) * LANES]
+        down_send[i] = down[:, i * LANES : (i + 1) * LANES]
     down_copies = tp_exchange(4, down_buf, lambda partner: down_send.at[partner])
     down_buf[tp] = down_send[tp]
     arrive(down_copies)
@@ -510,11 +562,18 @@
     anywhere = pl.BlockSpec(memory_space=pl.ANY)
     chunk_count = span // LANES
     dma = pltpu.SemaphoreType.DMA
+    half = ROWS // 2
     scratch = [
+        pltpu.SMEM(lengths.shape, jnp.int32),
+        pltpu.VMEM(tokens.shape, bf16),
+        pltpu.VMEM((1, LANES), f32),
+        pltpu.VMEM((1, heads), f32),
+        pltpu.VMEM((out_gain.shape[0] // LANES, LANES), f32),
+        pltpu.VMEM((ROWS, LANES), f32),
         pltpu.VMEM(w_query.shape, bf16),
         pltpu.VMEM(w_key.shape, bf16),
         pltpu.VMEM(w_value.shape, bf16),
-        pltpu.VMEM((block, heads), bf16),
+        pltpu.VMEM((heads, block), bf16),
         pltpu.VMEM(cache_keys.shape, bf16),
         pltpu.VMEM(cache_values.shape, bf16),
         pltpu.VMEM((chunk_count, batch, heads, LANES), f32),
@@ -522,11 +581,15 @@
         pltpu.VMEM(w_gate.shape, bf16),
         pltpu.VMEM(w_up.shape, bf16),
         pltpu.VMEM(w_down.shape, bf16),
-        pltpu.VMEM((tp_count, ROWS, LANES), f32),
-        pltpu.VMEM((kv_count, 3, ROWS, LANES), f32),
+        pltpu.VMEM((tp_count, ROWS, LANES), bf16),
+        pltpu.VMEM((tp_count, 1, LANES), f32),
+        pltpu.VMEM((kv_count, 2, ROWS, LANES), f32),
+        pltpu.VMEM((kv_count, 2, ROWS, LANES), f32),
+        pltpu.VMEM((tp_count, ROWS, LANES), bf16),
         pltpu.VMEM((tp_count, ROWS, LANES), f32),
         pltpu.VMEM((tp_count * 2 * ROWS, LANES), f32),
-        pltpu.VMEM((tp_count, 2 * ROWS, LANES), f32),
+        pltpu.VMEM((tp_count * 2 * ROWS, LANES), bf16),
+        pltpu.VMEM((tp_count, 2 * ROWS, LANES), bf16),
         pltpu.VMEM((kv_count, 2 * ROWS, LANES), f32),
         pltpu.VMEM((2 * ROWS, LANES), f32),
         pltpu.VMEM((tp_count, ROWS, columns // 2), bf16),
@@ -534,18 +597,18 @@
         pltpu.VMEM((kv_count, ROWS, LANES), f32),
         pltpu.VMEM((kv_count, ROWS, chunks[0][1] - chunks[0][0]), bf16),
         pltpu.VMEM((kv_count, ROWS, chunks[1][1] - chunks[1][0]), bf16),
-        pltpu.VMEM((tp_count, ROWS, LANES), f32),
-        pltpu.VMEM((tp_count, ROWS, LANES), f32),
-        dma((10 + chunk_count,)),
-        dma((5, tp_count - 1)),
-        dma((5, tp_count - 1)),
-        dma((5, kv_count - 1)),
-        dma((5, kv_count - 1)),
+        pltpu.VMEM((tp_count, half, LANES), f32),
+        pltpu.VMEM((tp_count, half, LANES), f32),
+        dma((16 + chunk_count,)),
+        dma((6, tp_count - 1)),
+        dma((6, tp_count - 1)),
+        dma((6, kv_count - 1)),
+        dma((6, kv_count - 1)),
     ]
     return pl.pallas_call(
         functools.partial(layer_kernel, kv_count, tp_count),
-        out_shape=jax.ShapeDtypeStruct(tokens.shape, bf16),
-        in_specs=[pl.BlockSpec(memory_space=pltpu.SMEM)] + [in_vmem] * 5 + [anywhere] * 11,
+        out_shape=pltpu.VMEM(tokens.shape, bf16),
+        in_specs=[anywhere] * 17,
         out_specs=in_vmem,
         scratch_shapes=scratch,
         compiler_params=pltpu.CompilerParams(
@@ -562,7 +625,7 @@
         w_query,
         w_key,
         w_value,
-        w_forget,
+        w_forget.T,
         cache_keys,
         cache_values,
         cache_decay,

time: 43 us -> 38.1 us (0.89)
  local copies, waits for them, and re-layouts: 3.52 us -> 0.56 us
  Pallas kernels: 39.3 us -> 37.4 us
    unnamed x2 -> x1, local copies, waits for them, and re-layouts: 3.52 us -> 0.56 us
    pallas_call x1, Pallas kernels: 39.3 us -> 37.4 us  [kernel_layer(): pl.pallas_call(functools.partial(layer_kernel, kv_count, tp_count), out_s...]
where the time goes in v2:
time: 38.1 us; the launch traced here: 37.9 us
  Pallas kernels  37.4 us (98%)
  local copies, waits for them, and re-layouts  0.56 us (1%)
    pallas_call x1, Pallas kernels, kernel_layer(): pl.pallas_call(functools.partial(layer_kernel, kv_count, tp_count), out_s...  37.4 us

profile of v2, /device:TPU:0, one launch (start us, length us, event | category | flops | bytes accessed | tf_op | source)
XLA Modules:
  0.0 37.9 jit_solution(12164692363770056642)
XLA Ops:
  0.0 37.4 %decode_layer.1 = bf16[3,128]{1,0:T(4,128)(2,1)S(1)} custom-call(s32[3]{0:T(128)} %lengths_hbm.1, bf16[3,128]{1,0:T(4,128)(2,1)} %tokens_hbm.1, f32[1,128]{1,0:T(1,128)} %bitcast.7, f32[1,128]{1,0:T(1,128)} %bitcast.8, f32[1,32]{1,0:T(1,128)} %bitcast.9, f32[16,128]{1,0:T(8,128)} %bitcast.6, bf16[1024,256]{1,0:T(8,128)(2,1)} %w_query_hbm.1, ...), custom_call_target="tpu_custom_call" | custom-call | tf_op jit(solution)/shard_map/decode_layer/pallas_call | solution.py:608
  37.4 0.6 %copy.19 = bf16[3,128]{1,0:T(4,128)(2,1)} copy(bf16[3,128]{1,0:T(4,128)(2,1)S(1)} %decode_layer.1) | data formatting | bytes 1536
